TPU v7x, 512 devices: a whole 4x4x16 slice. The times are simulated.
512 devices in a mesh: sp: 16 (over y, x), tp: 32 (over z, core).
Axes of the slice: x: 4, y: 4, z: 16, core: 2. Of those that a mesh axis runs over, the one named last changes fastest.
Arguments:
- tokens: bfloat16 [32, 2048, 4096], P('tp', 'sp'), may hold values from -6 to 6
- latent_down_matrix: bfloat16 [4096, 512], P('tp'), may hold values from -0.09375 to 0.09375
- rope_weight: bfloat16 [4096, 64], P('tp'), may hold values from -0.09375 to 0.09375
- latent_norm_scale: float32 [512], replicated, may hold values from 0.1 to 1.9
- key_up_matrix: bfloat16 [512, 32, 128], P(None, 'tp'), may hold values from -0.25 to 0.25
- value_up_matrix: bfloat16 [512, 32, 128], P(None, 'tp'), may hold values from -0.25 to 0.25
- query: bfloat16 [32, 32, 192], P('sp', 'tp'), may hold values from -126 to 126
Outputs:
- plain_key_cache: bfloat16 [32, 2048, 32, 128], P('sp', None, 'tp')
- head_value_cache: bfloat16 [32, 2048, 32, 128], P('sp', None, 'tp')
- rotated_key_cache: bfloat16 [32, 2048, 64], P('sp')
- first_read: bfloat16 [32, 32, 128], P('sp', 'tp')
All inputs are finite; a program needn't handle non-finite values.
Results may differ from a plain program's by a relative error of at most 0.035.
Values may be sent and summed in bfloat16 or wider, within the bound.
No kernel may reach another device: no remote copies, remote signals or barrier semaphores. Data moves between devices by JAX's collectives and lax.ppermute only.
A program may use at most 64 MiB of HBM per device.

v0:
```python
import jax
import jax.numpy as jnp
from jax import lax
from jax.sharding import PartitionSpec as P


def rotate(part, positions):
    half = part.shape[-1] // 2
    freqs = 1.0 / 10000.0 ** (jnp.arange(half, dtype=jnp.float32) * 2.0 / part.shape[-1])
    angles = positions.astype(jnp.float32)[:, None] * freqs
    cosine = jnp.cos(angles)
    sine = jnp.sin(angles)
    first = part[..., :half]
    second = part[..., half:]
    return jnp.concatenate(
        [first * cosine - second * sine, second * cosine + first * sine], axis=-1
    )


def body(
    tokens,
    latent_down_matrix,
    rope_weight,
    latent_norm_scale,
    key_up_matrix,
    value_up_matrix,
    query,
):
    seq_count, span, width = tokens.shape
    flat = tokens.reshape(seq_count * span, width)
    lat_width = latent_down_matrix.shape[1]
    rope_width = rope_weight.shape[1]
    latent = jnp.dot(
        flat,
        lax.all_gather(latent_down_matrix, "tp", axis=0, tiled=True),
        preferred_element_type=jnp.float32,
    )
    rope = jnp.dot(
        flat,
        lax.all_gather(rope_weight, "tp", axis=0, tiled=True),
        preferred_element_type=jnp.float32,
    )
    scaled = latent * lax.rsqrt(jnp.mean(latent * latent, axis=-1, keepdims=True) + 1e-06)
    latent_normalized = (scaled * latent_norm_scale).astype(jnp.bfloat16)
    offset = lax.axis_index("sp") * span
    positions = offset + jnp.arange(span, dtype=jnp.int32)
    rope_key = rotate(rope.reshape(seq_count, span, rope_width), positions).astype(jnp.bfloat16)
    packed = jnp.concatenate(
        [latent_normalized.reshape(seq_count, span, lat_width), rope_key], axis=-1
    )
    heads = key_up_matrix.shape[1]
    key_width = key_up_matrix.shape[2]
    val_width = value_up_matrix.shape[2]
    head_width = key_width + val_width
    up_weight = jnp.concatenate([key_up_matrix, value_up_matrix], axis=-1).reshape(
        lat_width, heads * head_width
    )
    piece = lax.all_gather(packed, "tp", axis=0, tiled=True)
    lead = piece.shape[:-1]
    product = jnp.dot(
        piece[..., :lat_width].reshape(-1, lat_width), up_weight, preferred_element_type=jnp.float32
    ).astype(jnp.bfloat16)
    projected = jnp.concatenate(
        [product.reshape(lead + (heads * head_width,)), piece[..., lat_width:]], axis=-1
    )
    built = lax.all_to_all(projected, "sp", split_axis=0, concat_axis=1, tiled=True)
    kept, length = (built.shape[0], built.shape[1])
    per_head = built[..., : heads * head_width].reshape(kept, length, heads, head_width)
    plain_key_cache = per_head[..., :key_width]
    head_value_cache = per_head[..., key_width:]
    rotated_key_cache = built[..., heads * head_width :]
    query_plain = query[..., :key_width]
    rotated_query = rotate(
        query[..., key_width:].astype(jnp.float32), jnp.full((1,), length, jnp.int32)
    ).astype(jnp.bfloat16)
    factor = 1.0 / (key_width + rope_width) ** 0.5
    scores = jnp.einsum(
        "shd,slhd->shl", query_plain, plain_key_cache, preferred_element_type=jnp.float32
    )
    scores = scores + jnp.einsum(
        "ikg,ivg->ikv", rotated_query, rotated_key_cache, preferred_element_type=jnp.float32
    )
    scores = scores * factor
    weights = jnp.exp(scores - jnp.max(scores, axis=-1, keepdims=True))
    total = jnp.sum(weights, axis=-1, keepdims=True)
    mixed = jnp.einsum(
        "shl,slhd->shd",
        weights.astype(jnp.bfloat16),
        head_value_cache,
        preferred_element_type=jnp.float32,
    )
    first_read = (mixed / total).astype(jnp.bfloat16)
    return (plain_key_cache, head_value_cache, rotated_key_cache, first_read)


def solution(mesh):
    in_specs = (
        P("tp", "sp", None),
        P("tp", None),
        P("tp", None),
        P(),
        P(None, "tp", None),
        P(None, "tp", None),
        P("sp", "tp", None),
    )
    out_specs = (
        P("sp", None, "tp", None),
        P("sp", None, "tp", None),
        P("sp", None, None),
        P("sp", "tp", None),
    )
    return jax.shard_map(body, mesh=mesh, in_specs=in_specs, out_specs=out_specs, check_vma=False)
```

profile of v0, /device:TPU:7, one launch (start us, length us, event | category | flops | bytes accessed | tf_op | source)
XLA Modules:
  0.0 249.8 jit_solution(4746171671624144846)
XLA Ops:
  7.2 0.0 copy-start
  7.2 0.0 all-gather.3.cloned.1.call-start
  7.2 0.7 all-gather.3.cloned.1.call-update
  7.9 0.0 all-gather.5.cloned.1.call-start
  8.0 38.6 %all_gather.10 = bf16[4096,64]{0,1:T(8,128)(2,1)S(1)} all-gather(bf16[128,64]{0,1:T(8,128)(2,1)} %param.9), channel_id=1, replica_groups=mesh['sp'=16,'tp'=32] {'tp'}, dimensions={0}, use_global_device_ids=true | all-gather | bytes 540672 | tf_op jit(solution)/shard_map/all_gather | solution.py:40
  46.6 0.0 copy-done
  46.6 0.5 convolution_bitcast_fusion
  47.1 0.1 fusion.15
  47.2 0.1 copy.36
  47.3 0.1 copy.35
  47.5 0.0 copy-start.1
  47.5 41.4 %all-gather.3.cloned.1.call-done = bf16[4096,512]{1,0:T(8,128)(2,1)} async-done(((bf16[128,512]{1,0:T(8,128)(2,1)}), bf16[4096,512]{1,0:T(8,128)(2,1)}) %all-gather.3.cloned.1.call-update) | async-done | bytes 4194320 | tf_op jit(solution)/shard_map/all_gather | solution.py:35
  88.9 3.0 %multiply_reduce_fusion = (f32[128]{0:T(128)S(1)}, f32[128,512]{1,0:T(8,128)S(1)}) fusion(bf16[4096,512]{1,0:T(8,128)(2,1)} %all-gather.3.cloned.1.call-done, bf16[1,128,4096]{2,1,0:T(8,128)(2,1)S(1)} %copy-done), kind=kOutput, calls=%fused_computation.16 | convolution fusion | flops 537001856 | bytes 5505536 | tf_op jit(solution)/shard_map/dot_general | solution.py:33
  91.9 0.0 copy-done.1
  91.9 0.1 fusion.9
  92.0 0.1 pad_maximum_fusion.1
  92.1 0.8 copy.37
  92.9 0.0 all-gather.5.cloned.1.call-update
  92.9 70.9 %all-gather.5.cloned.1.call-done = bf16[32,128,576]{1,2,0:T(8,128)(2,1)} async-done(((bf16[1,128,576]{1,2,0:T(8,128)(2,1)}), bf16[32,128,576]{1,2,0:T(8,128)(2,1)}) %all-gather.5.cloned.1.call-update) | async-done | bytes 4718608 | tf_op jit(solution)/shard_map/all_gather | solution.py:58
  163.9 4.7 %slice.50 = bf16[32,128,512]{1,2,0:T(8,128)(2,1)} slice(bf16[32,128,576]{1,2,0:T(8,128)(2,1)} %all-gather.5.cloned.1.call-done), slice={[0:32], [0:128], [0:512]} | slice | bytes 8388608 | tf_op jit(solution)/shard_map/slice | solution.py:61
  168.5 0.0 copy-start.2
  168.5 0.0 copy-start.3
  168.5 6.5 %copy.49 = bf16[32,128,512]{2,1,0:T(8,128)(2,1)} copy(bf16[32,128,512]{1,2,0:T(8,128)(2,1)} %slice.50) | data formatting | bytes 8388608
  175.1 0.0 copy-done.2
  175.1 0.0 copy-done.3
  175.1 4.8 %convolution_convert_fusion = bf16[4096,256]{1,0:T(8,128)(2,1)} fusion(bf16[4096,512]{1,0:T(8,128)(2,1)} %bitcast.60, bf16[512,1,128]{2,0,1:T(8,128)(2,1)S(1)} %copy-done.2, bf16[512,1,128]{2,0,1:T(8,128)(2,1)S(1)} %copy-done.3), kind=kOutput, calls=%fused_computation | convolution fusion | flops 1075314688 | bytes 6553600 | tf_op jit(solution)/shard_map/dot_general | solution.py:60
  179.9 3.2 %copy.39 = bf16[32,128,256]{1,2,0:T(8,128)(2,1)S(1)} copy(bf16[32,128,256]{2,1,0:T(8,128)(2,1)} %bitcast.61) | data formatting | bytes 4194304 | tf_op jit(solution)/shard_map/reshape | solution.py:64
  183.1 1.1 slice.51
  184.2 1.7 pad_maximum_fusion
  185.9 0.0 copy-start.4
  185.9 6.8 %all-to-all-start = ((bf16[32,128,320]{1,2,0:T(8,128)(2,1)}), bf16[32,128,320]{1,2,0:T(8,128)(2,1)}, u32[]{:S(2)}, u32[]{:S(2)}) async-start(bf16[32,128,320]{1,2,0:T(8,128)(2,1)} %pad_maximum_fusion), calls=%async_computation | async-start | bytes 5242880 | tf_op jit(solution)/shard_map/all_to_all | solution.py:66
  192.8 0.0 copy-done.4
  192.8 0.1 fusion.27
  192.9 0.1 maximum_bitcast_fusion.2
  193.0 37.8 %all-to-all-done = bf16[32,128,320]{1,2,0:T(8,128)(2,1)} async-done(((bf16[32,128,320]{1,2,0:T(8,128)(2,1)}), bf16[32,128,320]{1,2,0:T(8,128)(2,1)}, u32[]{:S(2)}, u32[]{:S(2)}) %all-to-all-start) | async-done | bytes 2621472 | tf_op jit(solution)/shard_map/all_to_all | solution.py:66
  230.7 2.5 copy.62
  233.2 0.1 slice_bitcast_fusion
  233.4 0.8 slice.55
  234.2 1.4 fusion.34
  235.7 2.3 copy.41
  237.9 2.3 copy.42
  240.2 0.2 fusion.2
  240.4 1.2 fusion.23
  241.7 0.1 fusion.32
  241.8 0.2 fusion.20
  242.0 0.4 fusion
  242.4 0.6 fusion.26
  (6 shorter events, 0.1 us)
Async XLA Ops:
  7.2 39.4 %copy-start = (bf16[1,128,4096]{2,1,0:T(8,128)(2,1)S(1)}, bf16[1,128,4096]{2,1,0:T(8,128)(2,1)}, u32[]{:S(2)}) copy-start(bf16[1,128,4096]{2,1,0:T(8,128)(2,1)} %param.7) | copy-start | bytes 3145732
  7.2 81.7 %all-gather.3.cloned.1.call-start = ((), (), s32[]{:S(2)}) async-start(), calls=%async_computation.1 | async-start | bytes 4325376 | tf_op jit(solution)/shard_map/all_gather | solution.py:35
  7.9 155.9 %all-gather.5.cloned.1.call-start = ((), (), s32[]{:S(2)}) async-start(), calls=%async_computation.2 | async-start | bytes 4866048 | tf_op jit(solution)/shard_map/all_gather | solution.py:58
  47.5 44.4 %copy-start.1 = (f32[512]{0:T(512)S(1)}, f32[512]{0:T(512)}, u32[]{:S(2)}) copy-start(f32[512]{0:T(512)} %param.10) | copy-start | bytes 6148
  168.5 6.5 %copy-start.2 = (bf16[512,1,128]{2,0,1:T(8,128)(2,1)S(1)}, bf16[512,1,128]{2,0,1:T(8,128)(2,1)}, u32[]{:S(2)}) copy-start(bf16[512,1,128]{2,0,1:T(8,128)(2,1)} %param.12) | copy-start | bytes 393220
  168.5 6.5 %copy-start.3 = (bf16[512,1,128]{2,0,1:T(8,128)(2,1)S(1)}, bf16[512,1,128]{2,0,1:T(8,128)(2,1)}, u32[]{:S(2)}) copy-start(bf16[512,1,128]{2,0,1:T(8,128)(2,1)} %param.11) | copy-start | bytes 393220
  185.9 6.9 %copy-start.4 = (bf16[2,1,192]{2,0,1:T(2,128)(2,1)S(1)}, bf16[2,1,192]{2,0,1:T(2,128)(2,1)}, u32[]{:S(2)}) copy-start(bf16[2,1,192]{2,0,1:T(2,128)(2,1)} %param.13) | copy-start | bytes 2308
  185.9 44.8 %all-to-all-start = ((bf16[32,128,320]{1,2,0:T(8,128)(2,1)}), bf16[32,128,320]{1,2,0:T(8,128)(2,1)}, u32[]{:S(2)}, u32[]{:S(2)}) async-start(bf16[32,128,320]{1,2,0:T(8,128)(2,1)} %pad_maximum_fusion), calls=%async_computation | async-start | bytes 5242880 | tf_op jit(solution)/shard_map/all_to_all | solution.py:66
Sparse Core Ops, SparseCore 0:
  10.1 78.7 all-gather.2
  93.1 70.7 all-gather.4
where the time goes:
time: 253 us; the launch traced here: 250 us
  waiting for transfers between devices  151 us (60%)
  blocking collectives  38.6 us (15%)
  local copies, waits for them, and re-layouts  26 us (10%)
  between operations  14.2 us (6%)
  matrix products  10.1 us (4%)
  starting transfers between devices  6.91 us (3%)
  other arithmetic  3.23 us (1%)
    all_gather x1, waiting for transfers between devices, body(): piece = lax.all_gather(packed, 'tp', axis=0, tiled=True)  70.9 us
    all_gather x1, waiting for transfers between devices, body(): lax.all_gather(latent_down_matrix, 'tp', axis=0, tiled=True)  41.4 us
    all_gather x1, blocking collectives, body(): lax.all_gather(rope_weight, 'tp', axis=0, tiled=True)  38.6 us
    all_to_all x1, waiting for transfers between devices, body(): lax.all_to_all(projected, 'sp', split_axis=0, concat_axis=1, tiled=True)  37.8 us
    unnamed x13, local copies, waits for them, and re-layouts  11.1 us
    all_to_all x1, starting transfers between devices, body(): lax.all_to_all(projected, 'sp', split_axis=0, concat_axis=1, tiled=True)  6.84 us
  transfers between devices with their start and end apart: 3, of which 3 were waited for; matrix products, arithmetic and copies ran while one was open for 0% of the time, Pallas kernels for 0%

commit v1 on v0

v1 whole, which is shorter than its diff:
```python
import jax
import jax.numpy as jnp
import numpy as np
from jax import lax
from jax.experimental import pallas as pl
from jax.experimental.pallas import tpu as pltpu
from jax.sharding import PartitionSpec as P

PLACE = (
    (7, 3, 0, 12, 8, 11, 2, 6, 4, 15, 1, 10, 13, 5, 14, 9),
    (1, 10, 15, 6, 2, 4, 8, 12, 11, 0, 7, 3, 9, 14, 5, 13),
    (4, 15, 10, 14, 9, 1, 13, 5, 7, 3, 11, 0, 2, 6, 12, 8),
    (6, 2, 9, 1, 10, 14, 3, 7, 5, 13, 12, 8, 15, 4, 11, 0),
    (10, 1, 4, 2, 6, 15, 12, 8, 0, 11, 3, 7, 14, 9, 13, 5),
    (11, 0, 3, 5, 13, 7, 9, 14, 1, 10, 4, 15, 8, 12, 6, 2),
    (2, 6, 14, 10, 1, 9, 7, 3, 13, 5, 8, 12, 4, 15, 0, 11),
    (8, 12, 5, 3, 7, 13, 1, 10, 9, 14, 2, 6, 11, 0, 15, 4),
    (13, 5, 12, 0, 11, 8, 4, 15, 2, 6, 9, 14, 7, 3, 10, 1),
    (9, 14, 6, 15, 4, 2, 11, 0, 8, 12, 13, 5, 1, 10, 3, 7),
    (0, 11, 7, 13, 5, 3, 14, 9, 10, 1, 15, 4, 12, 8, 2, 6),
    (3, 7, 11, 8, 12, 0, 6, 2, 15, 4, 10, 1, 5, 13, 9, 14),
    (5, 13, 8, 11, 0, 12, 15, 4, 6, 2, 14, 9, 3, 7, 1, 10),
    (12, 8, 13, 7, 3, 5, 10, 1, 14, 9, 6, 2, 0, 11, 4, 15),
    (15, 4, 1, 9, 14, 10, 5, 13, 3, 7, 0, 11, 6, 2, 8, 12),
    (14, 9, 2, 4, 15, 6, 0, 11, 12, 8, 5, 13, 10, 1, 7, 3),
)

W_SCALE = 2.0**19
LAT_SCALE = 2.0**10
ROPE_SCALE = 2.0**4
VMEM = pl.BlockSpec(memory_space=pltpu.VMEM)
SMEM = pl.BlockSpec(memory_space=pltpu.SMEM)


def down_kernel(tab, tok, mine, other, gain, cos, sin, out):
    width = mine.shape[2]
    rows = tok.shape[0]
    lat = jnp.zeros((rows, width), jnp.float32)
    rope = jnp.zeros((rows, 64), jnp.float32)
    for half, w in enumerate((mine, other)):
        for j in range(0, 16, 2):
            x = jnp.concatenate(
                [
                    tok[:, pl.ds(pl.multiple_of(tab[16 * half + i], 128), 128)]
                    for i in (j, j + 1)
                ],
                axis=1,
            )
            lat += jnp.dot(
                x, w[j : j + 2, :128, :].reshape(256, width), preferred_element_type=jnp.float32
            )
            wr = jnp.concatenate(
                [
                    jnp.concatenate(
                        [w[i, 128:144, k * 128 : (k + 1) * 128] for k in range(4)], axis=0
                    )
                    for i in (j, j + 1)
                ],
                axis=1,
            )
            rope += lax.dot_general(
                x, wr, (((1,), (1,)), ((), ())), preferred_element_type=jnp.float32
            )
    lat = lat * (1.0 / W_SCALE)
    scaled = lat * lax.rsqrt(jnp.mean(lat * lat, axis=-1, keepdims=True) + 1e-06)
    out[0:128, :] = (scaled * gain[...]).astype(jnp.bfloat16)
    turned = jnp.transpose(rope * (1.0 / W_SCALE))
    first, second = turned[:32], turned[32:]
    c, s = cos[...], sin[...]
    a = (first * c - second * s).astype(jnp.bfloat16)
    b = (second * c + first * s).astype(jnp.bfloat16)
    out[128:144, :] = jnp.concatenate([a[:16], a[16:], b[:16], b[16:]], axis=1)


def up_kernel(tab, mine, other, wk, wv, qp, qt, keys, values, rot, read):
    wkv = jnp.concatenate([wk[...], wv[...]], axis=1)
    for half, y in enumerate((mine, other)):
        s = tab[16] if half == 0 else 1 - tab[16]
        for p in range(16):
            x = y[tab[p]]
            kv = jnp.dot(x[:128], wkv, preferred_element_type=jnp.float32).astype(jnp.bfloat16)
            keys[s, p * 128 : (p + 1) * 128, :] = kv[:, :128]
            values[s, p * 128 : (p + 1) * 128, :] = kv[:, 128:]
            for k in range(4):
                rot[s, k * 16 : (k + 1) * 16, p * 128 : (p + 1) * 128] = x[
                    128:144, k * 128 : (k + 1) * 128
                ]
        scores = lax.dot_general(
            qp[s], keys[s], (((1,), (1,)), ((), ())), preferred_element_type=jnp.float32
        )
        scores = scores + jnp.dot(qt[s], rot[s], preferred_element_type=jnp.float32)
        scores = scores * (1.0 / 192.0**0.5)
        weights = jnp.exp(scores - jnp.max(scores, axis=-1, keepdims=True))
        total = jnp.sum(weights, axis=-1, keepdims=True)
        mixed = jnp.dot(
            weights.astype(jnp.bfloat16), values[s], preferred_element_type=jnp.float32
        )
        read[s] = (mixed / total).astype(jnp.bfloat16)


def turn(positions, half):
    freqs = 1.0 / 10000.0 ** (jnp.arange(half, dtype=jnp.float32) / half)
    angles = freqs[:, None] * positions.astype(jnp.float32)[None, :]
    return jnp.cos(angles), jnp.sin(angles)


def body(tokens, down, rope_w, gain, key_up, value_up, query):
    place = np.array(PLACE)
    origin = np.zeros((16, 16), np.int32)
    for p in range(16):
        for q in range(16):
            origin[place[p][q]][p] = q
    col = lax.axis_index("sp")
    tp = lax.axis_index("tp")
    z, core = tp // 2, tp % 2
    both = ("sp", "tp")
    lines = [[2 * k + c for k in range(16)] for c in range(2)]
    swap = [(t, t ^ 1) for t in range(32)]

    packed = jnp.concatenate(
        [
            down,
            jnp.concatenate([rope_w.T[16 * k : 16 * (k + 1)] for k in range(4)], axis=1),
        ],
        axis=0,
    )
    packed = (packed.astype(jnp.float32) * W_SCALE).astype(jnp.float16)
    along = [
        (p * 32 + 2 * q + c, p * 32 + 2 * int(place[p][q]) + c)
        for p in range(16)
        for q in range(16)
        for c in range(2)
    ]
    moved = lax.ppermute(packed, both, along)
    mine = lax.all_gather(moved, "sp", axis=0).astype(jnp.bfloat16)
    other = lax.ppermute(mine, "tp", swap)

    chips = jnp.asarray(origin)[z]
    tab = jnp.concatenate([chips * 256 + core * 128, chips * 256 + (1 - core) * 128]).astype(
        jnp.int32
    )
    cos, sin = turn(col * 128 + jnp.arange(128, dtype=jnp.int32), 32)
    block = pl.pallas_call(
        down_kernel,
        out_shape=jax.ShapeDtypeStruct((144, 512), jnp.bfloat16),
        in_specs=[SMEM, VMEM, VMEM, VMEM, VMEM, VMEM, VMEM],
        out_specs=VMEM,
        cost_estimate=pl.CostEstimate(
            flops=2 * 128 * 4096 * 576, bytes_accessed=6 << 20, transcendentals=0
        ),
    )(tab, tokens[0], mine, other, gain.reshape(1, 512), cos, sin)

    level = jnp.concatenate(
        [jnp.full((128, 1), LAT_SCALE, jnp.float32), jnp.full((16, 1), ROPE_SCALE, jnp.float32)]
    )
    block = (block.astype(jnp.float32) * level).astype(jnp.float16)
    across = [
        (p * 32 + 2 * q + c, q * 32 + 2 * int(place[p][q]) + c)
        for p in range(16)
        for q in range(16)
        for c in range(2)
    ]
    block = lax.ppermute(block, both, across)
    line = lax.all_gather(block, "tp", axis=0, axis_index_groups=lines)
    line = (line.astype(jnp.float32) * (1.0 / level)).astype(jnp.bfloat16)
    pair = lax.ppermute(line, "tp", swap)

    query_plain = query[..., :128]
    last = query[..., 128:].astype(jnp.float32)
    qc, qs = turn(jnp.full((1,), 2048, jnp.int32), 32)
    qc, qs = qc[:, 0], qs[:, 0]
    first, second = last[..., :32], last[..., 32:]
    query_turned = jnp.concatenate(
        [first * qc - second * qs, second * qc + first * qs], axis=-1
    ).astype(jnp.bfloat16)
    tab2 = jnp.concatenate([jnp.asarray(place.T)[col], core[None]]).astype(jnp.int32)
    keys, values, rot, read = pl.pallas_call(
        up_kernel,
        out_shape=(
            jax.ShapeDtypeStruct((2, 2048, 128), jnp.bfloat16),
            jax.ShapeDtypeStruct((2, 2048, 128), jnp.bfloat16),
            jax.ShapeDtypeStruct((2, 64, 2048), jnp.bfloat16),
            jax.ShapeDtypeStruct((2, 1, 128), jnp.bfloat16),
        ),
        in_specs=[SMEM] + [VMEM] * 6,
        out_specs=(VMEM,) * 4,
        cost_estimate=pl.CostEstimate(
            flops=2 * 4096 * 512 * 256, bytes_accessed=8 << 20, transcendentals=4096
        ),
    )(tab2, line, pair, key_up[:, 0], value_up[:, 0], query_plain, query_turned)
    return (
        keys[:, :, None, :],
        values[:, :, None, :],
        jnp.swapaxes(rot, 1, 2),
        read,
    )


def solution(mesh):
    in_specs = (
        P("tp", "sp", None),
        P("tp", None),
        P("tp", None),
        P(),
        P(None, "tp", None),
        P(None, "tp", None),
        P("sp", "tp", None),
    )
    out_specs = (
        P("sp", None, "tp", None),
        P("sp", None, "tp", None),
        P("sp", None, None),
        P("sp", "tp", None),
    )
    return jax.shard_map(body, mesh=mesh, in_specs=in_specs, out_specs=out_specs, check_vma=False)
```

time: 253 us -> 154 us (0.61); the launches traced: 250 us -> 154 us
  waiting for transfers between devices: 151 us -> 15.3 us
  blocking collectives: 38.6 us -> 82.4 us
  starting transfers between devices: 6.91 us -> 35.2 us
  local copies, waits for them, and re-layouts: 26 us -> 3.16 us
  between operations: 14.2 us -> 0.78 us
  Pallas kernels: 0 us -> 10.2 us
  matrix products: 10.1 us -> 0 us
  other arithmetic: 3.23 us -> 6.77 us
    all_gather x2 -> x0, waiting for transfers between devices: 112 us -> none  [the longest x1 70.9 us: body(): piece = lax.all_gather(packed, 'tp', axis=0, tiled=True)]
    all_gather x1 -> x2, blocking collectives: 38.6 us -> 82.4 us  [the longest x1 53.1 us: body(): line = lax.all_gather(block, 'tp', axis=0, axis_index_groups=lines)]
    all_to_all x1 -> x0, waiting for transfers between devices: 37.8 us -> none  [body(): lax.all_to_all(projected, 'sp', split_axis=0, concat_axis=1, tiled=True)]
    ppermute x0 -> x4, starting transfers between devices: none -> 35.2 us  [the longest x1 11.5 us: body(): moved = lax.ppermute(packed, both, along)]
    ppermute x0 -> x4, waiting for transfers between devices: none -> 15.3 us  [the longest x1 7.08 us: body(): block = lax.ppermute(block, both, across)]
    pallas_call x0 -> x2, Pallas kernels: none -> 10.2 us  [the longest x1 5.68 us: body(): pl.pallas_call(up_kernel, out_shape=(jax.ShapeDtypeStruct((2, 2048, 128),...]
    dot_general x6 -> x0, matrix products: 10.1 us -> none  [the longest x1 4.79 us: body(): jnp.dot(piece[..., :lat_width].reshape(-1, lat_width), up_weight, preferr...]
    unnamed x13 -> x10, local copies, waits for them, and re-layouts: 11.1 us -> 1.72 us
  transfers between devices with their start and end apart: 3 -> 4, of which waited for: 3 -> 4; matrix products, arithmetic and copies ran while one was open for 0% -> 3% of each run, Pallas kernels for 0% -> 0%
where the time goes in v1:
time: 154 us
  blocking collectives  82.4 us (54%)
  starting transfers between devices  35.2 us (23%)
  waiting for transfers between devices  15.3 us (10%)
  Pallas kernels  10.2 us (7%)
  other arithmetic  6.77 us (4%)
  local copies, waits for them, and re-layouts  3.16 us (2%)
    all_gather x1, blocking collectives, body(): line = lax.all_gather(block, 'tp', axis=0, axis_index_groups=lines)  53.1 us
    all_gather x1, blocking collectives, body(): mine = lax.all_gather(moved, 'sp', axis=0).astype(jnp.bfloat16)  29.4 us
    ppermute x1, starting transfers between devices, body(): moved = lax.ppermute(packed, both, along)  11.5 us
    ppermute x1, starting transfers between devices, body(): pair = lax.ppermute(line, 'tp', swap)  10.6 us
    ppermute x1, waiting for transfers between devices, body(): block = lax.ppermute(block, both, across)  7.08 us
    ppermute x1, starting transfers between devices, body(): other = lax.ppermute(mine, 'tp', swap)  6.97 us
    ppermute x1, starting transfers between devices, body(): block = lax.ppermute(block, both, across)  6.15 us
    pallas_call x1, Pallas kernels, body(): pl.pallas_call(up_kernel, out_shape=(jax.ShapeDtypeStruct((2, 2048, 128),...  5.68 us
  transfers between devices with their start and end apart: 4, of which 4 were waited for; matrix products, arithmetic and copies ran while one was open for 3% of the time, Pallas kernels for 0%

profile of v1, /device:TPU:7, one launch (start us, length us, event | category | flops | bytes accessed | tf_op | source)
XLA Modules:
  0.0 153.8 jit_solution(8797240073404991203)
XLA Ops:
  0.6 0.7 fusion.1
  1.4 0.9 multiply_convert_fusion.1
  2.3 11.5 %collective-permute-start = (f16[144,512]{1,0:T(8,128)(2,1)S(1)}, f16[144,512]{1,0:T(8,128)(2,1)S(1)}, u32[]{:S(2)}, u32[]{:S(2)}) collective-permute-start(f16[144,512]{1,0:T(8,128)(2,1)S(1)} %multiply_convert_fusion.1), channel_id=1, source_target_pairs={{0,14},{1,15},{2,6},{3,7},{4,0},{5,1},{6,24},{7,25},{8,16},{9,17},... | collective-permute-start | bytes 442376 | tf_op jit(solution)/shard_map/ppermute | solution.py:134
  13.8 4.3 %collective-permute-done = f16[144,512]{1,0:T(8,128)(2,1)S(1)} collective-permute-done((f16[144,512]{1,0:T(8,128)(2,1)S(1)}, f16[144,512]{1,0:T(8,128)(2,1)S(1)}, u32[]{:S(2)}, u32[]{:S(2)}) %collective-permute-start) | collective-permute-done | bytes 147488 | tf_op jit(solution)/shard_map/ppermute | solution.py:134
  18.2 29.4 %all-gather.4 = f16[2304,512]{1,0:T(8,128)(2,1)S(1)} all-gather(f16[144,512]{1,0:T(8,128)(2,1)S(1)} %collective-permute-done), channel_id=2, replica_groups=mesh['sp'=16,'tp'=32] {'sp'}, dimensions={0}, use_global_device_ids=true | all-gather | bytes 2506752 | tf_op jit(solution)/shard_map/all_gather | solution.py:135
  47.5 0.4 convert_element_type.41
  48.0 0.0 copy-start.1
  48.0 7.0 %collective-permute-start.1 = (bf16[16,144,512]{2,1,0:T(8,128)(2,1)S(1)}, bf16[16,144,512]{2,1,0:T(8,128)(2,1)}, u32[]{:S(2)}, u32[]{:S(2)}) collective-permute-start(bf16[16,144,512]{2,1,0:T(8,128)(2,1)S(1)} %bitcast.23), channel_id=1, source_target_pairs={{0,1},{1,0},{2,3},{3,2},{4,5},{5,4},{6,7},{7,6},{8,9},{9,8},{10,11... | collective-permute-start | bytes 7077896 | tf_op jit(solution)/shard_map/ppermute | solution.py:136
  55.0 0.7 add_bitcast_fusion.1
  55.7 0.6 pad_add_fusion.1.tab
  56.3 0.8 multiply_sine_fusion
  57.1 2.2 %collective-permute-done.1.other = bf16[16,144,512]{2,1,0:T(8,128)(2,1)} collective-permute-done((bf16[16,144,512]{2,1,0:T(8,128)(2,1)S(1)}, bf16[16,144,512]{2,1,0:T(8,128)(2,1)}, u32[]{:S(2)}, u32[]{:S(2)}) %collective-permute-start.1) | collective-permute-done | bytes 2359328 | tf_op jit(solution)/shard_map/ppermute | solution.py:136
  59.2 0.0 copy-done.1
  59.2 0.0 copy-start.3
  59.2 4.5 %shard_map.120 = bf16[144,512]{1,0:T(8,128)(2,1)} custom-call(s32[32]{0:T(128)} %pad_add_fusion.1.tab, bf16[128,4096]{1,0:T(8,128)(2,1)} %bitcast.25, bf16[16,144,512]{2,1,0:T(8,128)(2,1)} %bitcast.24, bf16[16,144,512]{2,1,0:T(8,128)(2,1)} %collective-permute-done.1.other, f32[1,512]{1,0:T(1,128)} %bitcast.29, f32[32,128]{1,0:T(8,128)} %get-tuple-element.25.cos, ...), custom_call_target="tpu_custom_call" | custom-call | flops 603979776 | bytes 6291456 | tf_op jit(solution)/shard_map/pallas_call | solution.py:143
  63.7 0.0 copy-done.3
  63.7 0.0 copy-start.2
  63.7 1.0 multiply_convert_fusion
  64.8 6.2 %collective-permute-start.2 = (f16[144,512]{1,0:T(8,128)(2,1)S(1)}, f16[144,512]{1,0:T(8,128)(2,1)S(1)}, u32[]{:S(2)}, u32[]{:S(2)}) collective-permute-start(f16[144,512]{1,0:T(8,128)(2,1)S(1)} %multiply_convert_fusion), channel_id=1, source_target_pairs={{0,14},{1,15},{2,38},{3,39},{4,64},{5,65},{6,120},{7,121},{8,144},... | collective-permute-start | bytes 442376 | tf_op jit(solution)/shard_map/ppermute | solution.py:163
  70.9 7.1 %collective-permute-done.2 = f16[144,512]{1,0:T(8,128)(2,1)S(1)} collective-permute-done((f16[144,512]{1,0:T(8,128)(2,1)S(1)}, f16[144,512]{1,0:T(8,128)(2,1)S(1)}, u32[]{:S(2)}, u32[]{:S(2)}) %collective-permute-start.2) | collective-permute-done | bytes 147488 | tf_op jit(solution)/shard_map/ppermute | solution.py:163
  78.0 53.1 %all-gather.5 = f16[2304,512]{1,0:T(8,128)(2,1)S(1)} all-gather(f16[144,512]{1,0:T(8,128)(2,1)S(1)} %collective-permute-done.2), channel_id=3, replica_groups={{0,2,4,6,8,10,12,14,16,18,20,22,24,26,28,30},{1,3,5,7,9,11,13,15,17,19,..., dimensions={0}, use_global_device_ids=true | all-gather | bytes 2506752 | tf_op jit(solution)/shard_map/all_gather | solution.py:164
  131.1 0.0 copy-done.2
  131.1 0.0 slice-start
  131.1 0.0 slice-start.1
  131.1 1.0 fusion.mine
  132.1 0.0 copy-start
  132.1 10.6 %collective-permute-start.3 = (bf16[16,144,512]{2,1,0:T(8,128)(2,1)S(1)}, bf16[16,144,512]{2,1,0:T(8,128)(2,1)}, u32[]{:S(2)}, u32[]{:S(2)}) collective-permute-start(bf16[16,144,512]{2,1,0:T(8,128)(2,1)S(1)} %fusion.mine), channel_id=1, source_target_pairs={{0,1},{1,0},{2,3},{3,2},{4,5},{5,4},{6,7},{7,6},{8,9},{9,8},{10,11... | collective-permute-start | bytes 7077896 | tf_op jit(solution)/shard_map/ppermute | solution.py:166
  142.7 0.0 slice-done
  142.7 0.5 copy.18.qp
  143.2 0.7 dynamic-slice_bitcast_fusion
  143.9 0.6 pad_add_fusion.tab
  144.5 0.0 slice-done.1
  144.5 0.1 subtract_convert_fusion
  144.6 0.7 pad_maximum_fusion.qt
  145.3 1.7 %collective-permute-done.3.other = bf16[16,144,512]{2,1,0:T(8,128)(2,1)} collective-permute-done((bf16[16,144,512]{2,1,0:T(8,128)(2,1)S(1)}, bf16[16,144,512]{2,1,0:T(8,128)(2,1)}, u32[]{:S(2)}, u32[]{:S(2)}) %collective-permute-start.3) | collective-permute-done | bytes 2359328 | tf_op jit(solution)/shard_map/ppermute | solution.py:166
  146.9 0.0 copy-done
  146.9 5.7 %shard_map.121 = (bf16[2,2048,128]{2,1,0:T(8,128)(2,1)}, bf16[2,2048,128]{2,1,0:T(8,128)(2,1)}, bf16[2,64,2048]{2,1,0:T(8,128)(2,1)}, bf16[2,1,128]{2,1,0:T(2,128)(2,1)}) custom-call(s32[17]{0:T(128)} %pad_add_fusion.tab, bf16[16,144,512]{2,1,0:T(8,128)(2,1)} %copy-done, bf16[16,144,512]{2,1,0:T(8,128)(2,1)} %collective-permute-done.3.other, ...), custom_call_target="tpu_custom_call" | custom-call | flops 1073741824 | bytes 8388608 | tf_op jit(solution)/shard_map/pallas_call | solution.py:177
  152.6 1.2 copy.17
  (4 shorter events, 0.1 us)
Async XLA Ops:
  2.3 15.9 %collective-permute-start = (f16[144,512]{1,0:T(8,128)(2,1)S(1)}, f16[144,512]{1,0:T(8,128)(2,1)S(1)}, u32[]{:S(2)}, u32[]{:S(2)}) collective-permute-start(f16[144,512]{1,0:T(8,128)(2,1)S(1)} %multiply_convert_fusion.1), channel_id=1, source_target_pairs={{0,14},{1,15},{2,6},{3,7},{4,0},{5,1},{6,24},{7,25},{8,16},{9,17},... | collective-permute-start | bytes 442376 | tf_op jit(solution)/shard_map/ppermute | solution.py:134
  48.0 11.3 %copy-start.1 = (bf16[2304,512]{1,0:T(8,128)(2,1)}, bf16[2304,512]{1,0:T(8,128)(2,1)S(1)}, u32[]{:S(2)}) copy-start(bf16[2304,512]{1,0:T(8,128)(2,1)S(1)} %convert_element_type.41) | copy-start | bytes 7077892
  48.0 11.2 %collective-permute-start.1 = (bf16[16,144,512]{2,1,0:T(8,128)(2,1)S(1)}, bf16[16,144,512]{2,1,0:T(8,128)(2,1)}, u32[]{:S(2)}, u32[]{:S(2)}) collective-permute-start(bf16[16,144,512]{2,1,0:T(8,128)(2,1)S(1)} %bitcast.23), channel_id=1, source_target_pairs={{0,1},{1,0},{2,3},{3,2},{4,5},{5,4},{6,7},{7,6},{8,9},{9,8},{10,11... | collective-permute-start | bytes 7077896 | tf_op jit(solution)/shard_map/ppermute | solution.py:136
  59.2 4.5 %copy-start.3 = (f32[144]{0:T(256)S(1)}, f32[144]{0:T(256)}, u32[]{:S(2)}) copy-start(f32[144]{0:T(256)} %constant.58.clone.1) | copy-start | bytes 1732
  63.7 67.3 %copy-start.2 = (f32[144]{0:T(256)S(1)}, f32[144]{0:T(256)}, u32[]{:S(2)}) copy-start(f32[144]{0:T(256)} %constant.59.clone.1) | copy-start | bytes 1732
  64.8 13.2 %collective-permute-start.2 = (f16[144,512]{1,0:T(8,128)(2,1)S(1)}, f16[144,512]{1,0:T(8,128)(2,1)S(1)}, u32[]{:S(2)}, u32[]{:S(2)}) collective-permute-start(f16[144,512]{1,0:T(8,128)(2,1)S(1)} %multiply_convert_fusion), channel_id=1, source_target_pairs={{0,14},{1,15},{2,38},{3,39},{4,64},{5,65},{6,120},{7,121},{8,144},... | collective-permute-start | bytes 442376 | tf_op jit(solution)/shard_map/ppermute | solution.py:163
  131.1 11.6 %slice-start = ((bf16[2,1,192]{2,0,1:T(2,128)(2,1)}), bf16[2,1,128]{2,0,1:T(2,128)(2,1)S(1)}, s32[]{:S(2)}) async-start(bf16[2,1,192]{2,0,1:T(2,128)(2,1)} %param.15), calls=%async_computation | async-start | bytes 1024 | tf_op jit(solution)/shard_map/slice | solution.py:168
  131.1 13.4 %slice-start.1 = ((bf16[2,1,192]{2,0,1:T(2,128)(2,1)}), bf16[2,1,64]{2,0,1:T(2,128)(2,1)S(1)}, s32[]{:S(2)}) async-start(bf16[2,1,192]{2,0,1:T(2,128)(2,1)} %param.15), calls=%async_computation.1 | async-start | bytes 1024 | tf_op jit(solution)/shard_map/slice | solution.py:169
  132.1 14.9 %copy-start = (bf16[16,144,512]{2,1,0:T(8,128)(2,1)}, bf16[16,144,512]{2,1,0:T(8,128)(2,1)S(1)}, u32[]{:S(2)}) copy-start(bf16[16,144,512]{2,1,0:T(8,128)(2,1)S(1)} %fusion.mine) | copy-start | bytes 7077892
  132.1 14.9 %collective-permute-start.3 = (bf16[16,144,512]{2,1,0:T(8,128)(2,1)S(1)}, bf16[16,144,512]{2,1,0:T(8,128)(2,1)}, u32[]{:S(2)}, u32[]{:S(2)}) collective-permute-start(bf16[16,144,512]{2,1,0:T(8,128)(2,1)S(1)} %fusion.mine), channel_id=1, source_target_pairs={{0,1},{1,0},{2,3},{3,2},{4,5},{5,4},{6,7},{7,6},{8,9},{9,8},{10,11... | collective-permute-start | bytes 7077896 | tf_op jit(solution)/shard_map/ppermute | solution.py:166
